TPU v7x, 128 devices: a whole 4x4x4 slice. The times are simulated.
128 devices in a mesh: fs: 16 (over z, y), tp: 8 (over x, core).
Axes of the slice: x: 4, y: 4, z: 4, core: 2. Of those that a mesh axis runs over, the one named last changes fastest.
Arguments:
- normed_input: bfloat16 [24576, 2048], P(('fs', 'tp')), may hold values from -6 to 6
- pre_act: bfloat16 [24576, 8192], P('fs', 'tp'), may hold values from -6 to 6
- out_grad: bfloat16 [24576, 2048], P(('fs', 'tp')), may hold values from -24 to 24
- up_weight: bfloat16 [2048, 8192], P('fs', 'tp'), may hold values from -0.125 to 0.125
- down_weight: bfloat16 [8192, 2048], P('tp', 'fs'), may hold values from -0.0625 to 0.0625
Outputs:
- input_grad: bfloat16 [24576, 2048], P(('fs', 'tp'))
- up_grad: float32 [2048, 8192], P('fs', 'tp')
- down_grad: float32 [8192, 2048], P('tp', 'fs')
All inputs are finite; a program needn't handle non-finite values.
Results may differ from a plain program's by a relative error of at most 0.014.
Values may be sent and summed in bfloat16 or wider, within the bound.
A program may use at most 128 MiB of HBM per device.

v0:
```python
import jax
import jax.numpy as jnp
from jax import lax
from jax.sharding import PartitionSpec as P


def sent_together(arrays, axis, dim, along):
    ends, at = ([], 0)
    for a in arrays[:-1]:
        at += a.shape[along]
        ends.append(at)
    both = jnp.concatenate(arrays, axis=along)
    return tuple(jnp.split(lax.all_gather(both, axis, axis=dim, tiled=True), ends, axis=along))


def cut_along(x, dim, count):
    before, after = (x.shape[:dim], x.shape[dim + 1 :])
    return jnp.moveaxis(x.reshape(*before, count, -1, *after), dim, 0)


def sum_at_owner(x, axis, dim):
    tiles = cut_along(x, dim, lax.axis_size(axis))
    arrived = lax.all_to_all(tiles, axis, split_axis=0, concat_axis=0, tiled=True)
    return arrived.astype(jnp.float32).sum(axis=0)


def local(normed_input, pre_act, out_grad, up_weight, down_weight):
    rows_all, grad_rows = sent_together((normed_input, out_grad), "tp", 0, 1)
    active = jnp.maximum(pre_act.astype(jnp.float32), 0.0)
    hidden = (active * active).astype(jnp.bfloat16)
    width = pre_act.shape[1]
    columns = grad_rows
    hidden_grad = jnp.dot(
        columns,
        lax.all_gather(down_weight, "fs", axis=1, tiled=True).T,
        preferred_element_type=jnp.float32,
    )
    pre_grad = (2.0 * active * hidden_grad).astype(jnp.bfloat16)
    partial_value = jnp.dot(
        pre_grad,
        lax.all_gather(up_weight, "fs", axis=0, tiled=True).T,
        preferred_element_type=jnp.float32,
    )
    rounded = lax.optimization_barrier(partial_value.astype(jnp.bfloat16))
    summed = sum_at_owner(rounded.astype(jnp.float32).astype(jnp.bfloat16), "tp", 0)
    input_grad = summed.astype(jnp.bfloat16)
    columns = rows_all
    both = lax.psum_scatter(
        jnp.concatenate(
            [
                jnp.dot(columns.T, pre_grad, preferred_element_type=jnp.float32),
                jnp.dot(grad_rows.T, hidden, preferred_element_type=jnp.float32),
            ],
            axis=1,
        ).astype(jnp.bfloat16),
        "fs",
        scatter_dimension=0,
        tiled=True,
    ).astype(jnp.float32)
    up_grad = both[:, :width]
    down_grad = both[:, width:].T
    up_grad, down_grad = (up_grad, down_grad)
    return (input_grad, up_grad, down_grad)


def solution(mesh):
    placed = (
        P(("fs", "tp"), None),
        P("fs", "tp"),
        P(("fs", "tp"), None),
        P("fs", "tp"),
        P("tp", "fs"),
    )
    return jax.shard_map(
        local,
        mesh=mesh,
        in_specs=placed,
        out_specs=(P(("fs", "tp"), None), P("fs", "tp"), P("tp", "fs")),
        check_vma=False,
    )
```

profile of v0, /device:TPU:1, one launch (start us, length us, event | category | flops | bytes accessed | tf_op | source)
XLA Modules:
  0.0 293.3 jit_solution(11470290909760394026)
XLA Ops:
  7.2 0.0 all-gather.4.cloned.1.call-start
  7.2 2.7 pad_maximum_fusion.1
  9.9 0.0 all-gather.4.cloned.1.call-update
  9.9 0.0 all-gather.6.cloned.1.call-start
  10.0 0.7 all-gather.6.cloned.1.call-update
  10.7 0.0 all-gather.8.cloned.1.call-start
  10.7 0.7 all-gather.8.cloned.1.call-update
  11.4 0.0 copy-start.1
  11.4 0.0 reduce-scatter.4.cloned.1.call-start
  11.5 69.5 %all-gather.4.cloned.1.call-done = bf16[1536,4096]{1,0:T(8,128)(2,1)} async-done(((bf16[192,4096]{1,0:T(8,128)(2,1)}), bf16[1536,4096]{1,0:T(8,128)(2,1)}) %all-gather.4.cloned.1.call-update) | async-done | bytes 12582928 | tf_op jit(solution)/shard_map/all_gather | solution.py:13
  80.9 11.6 %fusion.8 = bf16[2048,1024]{0,1:T(8,128)(2,1)} fusion(bf16[1536,4096]{1,0:T(8,128)(2,1)} %all-gather.4.cloned.1.call-done, bf16[1536,1024]{1,0:T(8,128)(2,1)} %param.6), kind=kOutput, calls=%fused_computation.11 | convolution fusion | flops 6450839552 | bytes 13631488 | tf_op jit(solution)/shard_map/dot_general | solution.py:52
  92.6 46.1 %all-gather.6.cloned.1.call-done = bf16[1024,2048]{1,0:T(8,128)(2,1)} async-done(((bf16[1024,128]{1,0:T(8,128)(2,1)}), bf16[1024,2048]{1,0:T(8,128)(2,1)}) %all-gather.6.cloned.1.call-update) | async-done | bytes 4194320 | tf_op jit(solution)/shard_map/all_gather | solution.py:35
  138.7 0.0 copy-done.1
  138.7 0.0 copy-start
  138.7 10.3 %multiply_convert_fusion.1 = bf16[1536,1024]{1,0:T(8,128)(2,1)S(1)} fusion(bf16[1536,1024]{1,0:T(8,128)(2,1)S(1)} %copy-done.1, bf16[1024,2048]{1,0:T(8,128)(2,1)} %all-gather.6.cloned.1.call-done, bf16[1536,4096]{1,0:T(8,128)(2,1)} %all-gather.4.cloned.1.call-done), kind=kOutput, calls=%fused_computation.5 | convolution fusion | flops 6450315264 | bytes 16777216 | tf_op jit(solution)/shard_map/dot_general | solution.py:33
  149.0 0.0 copy-start.2
  149.0 1.7 copy-done.2
  150.7 0.0 copy-done
  150.7 8.4 %fusion.11 = bf16[2048,1024]{0,1:T(8,128)(2,1)} fusion(bf16[1536,1024]{1,0:T(8,128)(2,1)S(1)} %multiply_convert_fusion.1, bf16[1536,4096]{1,0:T(8,128)(2,1)S(1)} %copy-done), kind=kOutput, calls=%fused_computation.12 | convolution fusion | flops 6444548096 | bytes 13631488 | tf_op jit(solution)/shard_map/dot_general | solution.py:51
  159.1 8.4 %pad_maximum_fusion = bf16[2048,2048]{0,1:T(8,128)(2,1)} fusion(bf16[2048,1024]{0,1:T(8,128)(2,1)} %fusion.8, bf16[2048,1024]{0,1:T(8,128)(2,1)} %fusion.11), kind=kLoop, calls=%fused_computation | loop fusion | flops 16777216 | bytes 16777216 | tf_op jit(solution)/shard_map/concatenate | solution.py:49
  167.5 11.9 %copy.10 = bf16[2048,2048]{1,0:T(8,128)(2,1)} copy(bf16[2048,2048]{0,1:T(8,128)(2,1)} %pad_maximum_fusion) | data formatting | bytes 16777216
  179.4 0.0 copy-start.3
  179.4 0.0 reduce-scatter.4.cloned.1.call-update
  179.4 13.4 %all-gather.8.cloned.1.call-done = bf16[2048,1024]{1,0:T(8,128)(2,1)} async-done(((bf16[128,1024]{1,0:T(8,128)(2,1)}), bf16[2048,1024]{1,0:T(8,128)(2,1)}) %all-gather.8.cloned.1.call-update) | async-done | bytes 4194320 | tf_op jit(solution)/shard_map/all_gather | solution.py:41
  192.8 0.0 copy-done.3
  192.8 9.3 %convolution_convert_fusion = bf16[1536,2048]{1,0:T(8,128)(2,1)S(1)} fusion(bf16[1536,1024]{1,0:T(8,128)(2,1)S(1)} %copy-done.3, bf16[2048,1024]{1,0:T(8,128)(2,1)} %all-gather.8.cloned.1.call-done), kind=kOutput, calls=%fused_computation.1 | convolution fusion | flops 6445596672 | bytes 13631488 | tf_op jit(solution)/shard_map/dot_general | solution.py:39
  202.2 76.1 %all_to_all.5 = bf16[8,192,2048]{2,1,0:T(8,128)(2,1)} all-to-all(bf16[8,192,2048]{2,1,0:T(8,128)(2,1)S(1)} %bitcast.8), channel_id=1, replica_groups=mesh['fs'=16,'tp'=8] {'tp'}, dimensions={0} | all-to-all | bytes 12582912 | tf_op jit(solution)/shard_map/all_to_all | solution.py:23
  278.3 5.2 %reduce_sum.12 = bf16[192,2048]{1,0:T(8,128)(2,1)} reduce(bf16[8,192,2048]{2,1,0:T(8,128)(2,1)} %all_to_all.5, bf16[]{:T(256)} %constant.6.clone.1), dimensions={0}, to_apply=%region_0.0 | reduce | flops 2752512 | bytes 7077890 | tf_op jit(solution)/shard_map/reduce_sum | solution.py:24
  283.5 0.0 reduce-scatter.4.cloned.1.call-done
  283.5 1.3 copy.11
  284.8 0.1 convert_element_type.24
  284.9 0.8 slice_bitcast_fusion
  285.8 1.0 copy.9
  (1 shorter events, 0.0 us)
Async XLA Ops:
  7.2 73.8 %all-gather.4.cloned.1.call-start = ((), (), s32[]{:S(2)}) async-start(), calls=%async_computation.2 | async-start | bytes 14155776 | tf_op jit(solution)/shard_map/all_gather | solution.py:13
  9.9 128.8 %all-gather.6.cloned.1.call-start = ((), (), s32[]{:S(2)}) async-start(), calls=%async_computation.3 | async-start | bytes 4456448 | tf_op jit(solution)/shard_map/all_gather | solution.py:35
  10.7 182.1 %all-gather.8.cloned.1.call-start = ((), (), s32[]{:S(2)}) async-start(), calls=%async_computation.4 | async-start | bytes 4456448 | tf_op jit(solution)/shard_map/all_gather | solution.py:41
  11.4 127.3 %copy-start.1 = (bf16[1536,1024]{1,0:T(8,128)(2,1)S(1)}, bf16[1536,1024]{1,0:T(8,128)(2,1)}, u32[]{:S(2)}) copy-start(bf16[1536,1024]{1,0:T(8,128)(2,1)} %param.6) | copy-start | bytes 9437188
  11.4 272.0 %reduce-scatter.4.cloned.1.call-start = ((), (), s32[]{:S(2)}) async-start(), calls=%async_computation.5 | async-start | bytes 8912896
  138.7 12.0 %copy-start = (bf16[1536,4096]{1,0:T(8,128)(2,1)S(1)}, bf16[1536,4096]{1,0:T(8,128)(2,1)}, u32[]{:S(2)}) copy-start(bf16[1536,4096]{1,0:T(8,128)(2,1)} %all-gather.4.cloned.1.call-done) | copy-start | bytes 37748740
  149.0 1.7 copy-start.2
  179.4 13.4 %copy-start.3 = (bf16[1536,1024]{1,0:T(8,128)(2,1)S(1)}, bf16[1536,1024]{1,0:T(8,128)(2,1)}, u32[]{:S(2)}) copy-start(bf16[1536,1024]{1,0:T(8,128)(2,1)} %copy-done.2) | copy-start | bytes 9437188
Sparse Core Ops, SparseCore 0:
  10.1 70.8 all-gather.3
  83.0 55.6 all-gather.5
  140.8 51.9 all-gather.7
  196.1 84.5 reduce-scatter.3
where the time goes:
time: 294 us; the launch traced here: 293 us
  waiting for transfers between devices  130 us (44%)
  blocking collectives  76.1 us (26%)
  matrix products  39.6 us (13%)
  local copies, waits for them, and re-layouts  16.8 us (6%)
  other arithmetic  16.4 us (6%)
  between operations  13.8 us (5%)
    all_to_all x1, blocking collectives, sum_at_owner(): lax.all_to_all(tiles, axis, split_axis=0, concat_axis=0, tiled=True)  76.1 us
    all_gather x1, waiting for transfers between devices, sent_together(): lax.all_gather(both, axis, axis=dim, tiled=True)  69.5 us
    all_gather x1, waiting for transfers between devices, local(): lax.all_gather(down_weight, 'fs', axis=1, tiled=True)  46.1 us
    unnamed x11, local copies, waits for them, and re-layouts  15.9 us
    all_gather x1, waiting for transfers between devices, local(): lax.all_gather(up_weight, 'fs', axis=0, tiled=True)  13.4 us
    dot_general x1, matrix products, local(): jnp.dot(grad_rows.T, hidden, preferred_element_type=jnp.float32)  11.6 us
    dot_general x1, matrix products, local(): jnp.dot(columns, lax.all_gather(down_weight, 'fs', axis=1, tiled=True).T,...  10.3 us
    dot_general x1, matrix products, local(): jnp.dot(pre_grad, lax.all_gather(up_weight, 'fs', axis=0, tiled=True).T,...  9.33 us
  transfers between devices with their start and end apart: 4, of which 3 were waited for; matrix products, arithmetic and copies ran while one was open for 22% of the time, Pallas kernels for 0%

commit v1 on v0

--- a/solution.py
+++ b/solution.py
@@ -32,7 +32,9 @@
     columns = grad_rows
     hidden_grad = jnp.dot(
         columns,
-        lax.all_gather(down_weight, "fs", axis=1, tiled=True).T,
+        jnp.concatenate(
+            lax.all_to_all(jnp.stack([down_weight] * lax.axis_size("fs")), "fs", 0, 0), axis=1
+        ).T,
         preferred_element_type=jnp.float32,
     )
     pre_grad = (2.0 * active * hidden_grad).astype(jnp.bfloat16)

time: 294 us -> 236 us (0.80)
  waiting for transfers between devices: 130 us -> 59 us
  starting transfers between devices: 0.16 us -> 8.75 us
  local copies, waits for them, and re-layouts: 16.8 us -> 22.4 us
    all_gather x1 -> x0, waiting for transfers between devices: 46.1 us -> none  [local(): lax.all_gather(down_weight, 'fs', axis=1, tiled=True)]
    all_gather x1, waiting for transfers between devices: 13.4 us -> 0.29 us  [local(): lax.all_gather(up_weight, 'fs', axis=0, tiled=True)]
    all_gather x1, waiting for transfers between devices: 69.5 us -> 57.9 us  [sent_together(): lax.all_gather(both, axis, axis=dim, tiled=True)]
    all_to_all x0 -> x1, starting transfers between devices: none -> 8.64 us  [local(): lax.all_to_all(jnp.stack([down_weight] * lax.axis_size('fs')), 'fs', 0, 0)]
    unnamed x11 -> x12, local copies, waits for them, and re-layouts: 15.9 us -> 19.1 us
  transfers between devices with their start and end apart: 4 -> 4, of which waited for: 3 -> 2; matrix products, arithmetic and copies ran while one was open for 22% -> 30% of each run, Pallas kernels for 0% -> 0%
where the time goes in v1:
time: 236 us; the launch traced here: 235 us
  blocking collectives  74.6 us (32%)
  waiting for transfers between devices  59 us (25%)
  matrix products  39.7 us (17%)
  local copies, waits for them, and re-layouts  22.4 us (9%)
  other arithmetic  16.7 us (7%)
  between operations  13.8 us (6%)
  starting transfers between devices  8.75 us (4%)
    all_to_all x1, blocking collectives, sum_at_owner(): lax.all_to_all(tiles, axis, split_axis=0, concat_axis=0, tiled=True)  74.6 us
    all_gather x1, waiting for transfers between devices, sent_together(): lax.all_gather(both, axis, axis=dim, tiled=True)  57.9 us
    unnamed x12, local copies, waits for them, and re-layouts  19.1 us
    dot_general x1, matrix products, local(): jnp.dot(grad_rows.T, hidden, preferred_element_type=jnp.float32)  11.2 us
    dot_general x1, matrix products, local(): jnp.dot(columns, jnp.concatenate(lax.all_to_all(jnp.stack([down_weight] *...  10.4 us
    dot_general x1, matrix products, local(): jnp.dot(pre_grad, lax.all_gather(up_weight, 'fs', axis=0, tiled=True).T,...  9.32 us
    dot_general x1, matrix products, local(): jnp.dot(columns.T, pre_grad, preferred_element_type=jnp.float32)  8.76 us
    concatenate x1, other arithmetic, local(): jnp.concatenate([jnp.dot(columns.T, pre_grad, preferred_element_type=jnp....  8.71 us
  transfers between devices with their start and end apart: 4, of which 2 were waited for; matrix products, arithmetic and copies ran while one was open for 30% of the time, Pallas kernels for 0%

profile of v1, /device:TPU:1, one launch (start us, length us, event | category | flops | bytes accessed | tf_op | source)
XLA Modules:
  0.0 235.0 jit_solution(5433989493618534094)
XLA Ops:
  7.2 0.0 all-gather.3.cloned.1.call-start
  7.2 2.7 %pad_maximum_fusion.1 = bf16[192,4096]{1,0:T(8,128)(2,1)} fusion(bf16[192,2048]{1,0:T(8,128)(2,1)} %param.7, bf16[192,2048]{1,0:T(8,128)(2,1)} %param.5), kind=kLoop, calls=%fused_computation.14 | loop fusion | flops 3145728 | bytes 3145728 | tf_op jit(solution)/shard_map/concatenate | solution.py:12
  9.9 0.0 all-gather.3.cloned.1.call-update
  9.9 1.1 copy.11
  11.0 0.0 copy-start.1
  11.0 2.5 %stack.2 = bf16[16,1024,128]{1,2,0:T(8,128)(2,1)} broadcast(bf16[1024,128]{0,1:T(8,128)(2,1)S(1)} %copy.11), dimensions={1,2} | broadcast | bytes 4456448 | tf_op jit(solution)/shard_map/stack | solution.py:36
  13.6 8.6 %all-to-all-start = ((bf16[16,1024,128]{1,2,0:T(8,128)(2,1)}), bf16[16,1024,128]{1,2,0:T(8,128)(2,1)}, u32[]{:S(2)}, u32[]{:S(2)}) async-start(bf16[16,1024,128]{1,2,0:T(8,128)(2,1)} %stack.2), calls=%async_computation | async-start | bytes 8388608 | tf_op jit(solution)/shard_map/all_to_all | solution.py:36
  22.2 0.0 all-gather.5.cloned.1.call-start
  22.2 0.7 all-gather.5.cloned.1.call-update
  23.0 0.0 reduce-scatter.4.cloned.1.call-start
  23.0 57.9 %all-gather.3.cloned.1.call-done = bf16[1536,4096]{1,0:T(8,128)(2,1)} async-done(((bf16[192,4096]{1,0:T(8,128)(2,1)}), bf16[1536,4096]{1,0:T(8,128)(2,1)}) %all-gather.3.cloned.1.call-update) | async-done | bytes 12582928 | tf_op jit(solution)/shard_map/all_gather | solution.py:13
  80.9 0.0 copy-done.1
  80.9 11.2 %fusion.8 = bf16[2048,1024]{0,1:T(8,128)(2,1)} fusion(bf16[1536,4096]{1,0:T(8,128)(2,1)} %all-gather.3.cloned.1.call-done, bf16[1536,1024]{1,0:T(8,128)(2,1)S(1)} %copy-done.1), kind=kOutput, calls=%fused_computation.11 | convolution fusion | flops 6450839552 | bytes 13631488 | tf_op jit(solution)/shard_map/dot_general | solution.py:54
  92.2 0.0 all-to-all-done
  92.2 0.0 copy-start
  92.2 10.4 %multiply_convert_fusion.1 = bf16[1536,1024]{1,0:T(8,128)(2,1)S(1)} fusion(bf16[1536,1024]{1,0:T(8,128)(2,1)S(1)} %copy-done.1, bf16[1024,2048]{0,1:T(8,128)(2,1)} %bitcast.1, bf16[1536,4096]{1,0:T(8,128)(2,1)} %all-gather.3.cloned.1.call-done), kind=kOutput, calls=%fused_computation.5 | convolution fusion | flops 6450315264 | bytes 16777216 | tf_op jit(solution)/shard_map/dot_general | solution.py:33
  102.6 0.0 copy-start.2
  102.6 1.7 copy-done.2
  104.3 0.0 copy-done
  104.3 8.8 %fusion.11 = bf16[2048,1024]{0,1:T(8,128)(2,1)} fusion(bf16[1536,1024]{1,0:T(8,128)(2,1)S(1)} %multiply_convert_fusion.1, bf16[1536,4096]{1,0:T(8,128)(2,1)S(1)} %copy-done), kind=kOutput, calls=%fused_computation.12 | convolution fusion | flops 6444548096 | bytes 13631488 | tf_op jit(solution)/shard_map/dot_general | solution.py:53
  113.0 8.7 %pad_maximum_fusion = bf16[2048,2048]{0,1:T(8,128)(2,1)} fusion(bf16[2048,1024]{0,1:T(8,128)(2,1)} %fusion.8, bf16[2048,1024]{0,1:T(8,128)(2,1)} %fusion.11), kind=kLoop, calls=%fused_computation | loop fusion | flops 16777216 | bytes 16777216 | tf_op jit(solution)/shard_map/concatenate | solution.py:51
  121.8 12.4 %copy.13 = bf16[2048,2048]{1,0:T(8,128)(2,1)} copy(bf16[2048,2048]{0,1:T(8,128)(2,1)} %pad_maximum_fusion) | data formatting | bytes 16777216
  134.1 0.0 copy-start.3
  134.1 0.0 reduce-scatter.4.cloned.1.call-update
  134.2 0.3 all-gather.5.cloned.1.call-done
  134.5 1.6 copy-done.3
  136.0 9.3 %convolution_convert_fusion = bf16[1536,2048]{1,0:T(8,128)(2,1)S(1)} fusion(bf16[1536,1024]{1,0:T(8,128)(2,1)S(1)} %copy-done.3, bf16[2048,1024]{1,0:T(8,128)(2,1)} %all-gather.5.cloned.1.call-done), kind=kOutput, calls=%fused_computation.1 | convolution fusion | flops 6445596672 | bytes 13631488 | tf_op jit(solution)/shard_map/dot_general | solution.py:41
  145.4 74.6 %all_to_all.10 = bf16[8,192,2048]{2,1,0:T(8,128)(2,1)} all-to-all(bf16[8,192,2048]{2,1,0:T(8,128)(2,1)S(1)} %bitcast.11), channel_id=1, replica_groups=mesh['fs'=16,'tp'=8] {'tp'}, dimensions={0} | all-to-all | bytes 12582912 | tf_op jit(solution)/shard_map/all_to_all | solution.py:23
  220.0 5.2 %reduce_sum.12 = bf16[192,2048]{1,0:T(8,128)(2,1)} reduce(bf16[8,192,2048]{2,1,0:T(8,128)(2,1)} %all_to_all.10, bf16[]{:T(256)} %constant.6.clone.1), dimensions={0}, to_apply=%region_0.0 | reduce | flops 2752512 | bytes 7077890 | tf_op jit(solution)/shard_map/reduce_sum | solution.py:24
  225.2 0.0 reduce-scatter.4.cloned.1.call-done
  225.2 1.3 copy.14
  226.5 0.1 convert_element_type.24
  226.7 0.8 slice_bitcast_fusion
  227.5 1.0 copy.12
  (1 shorter events, 0.0 us)
Async XLA Ops:
  7.2 73.8 %all-gather.3.cloned.1.call-start = ((), (), s32[]{:S(2)}) async-start(), calls=%async_computation.3 | async-start | bytes 14155776 | tf_op jit(solution)/shard_map/all_gather | solution.py:13
  11.0 69.9 %copy-start.1 = (bf16[1536,1024]{1,0:T(8,128)(2,1)S(1)}, bf16[1536,1024]{1,0:T(8,128)(2,1)}, u32[]{:S(2)}) copy-start(bf16[1536,1024]{1,0:T(8,128)(2,1)} %param.6) | copy-start | bytes 9437188
  13.6 78.6 %all-to-all-start = ((bf16[16,1024,128]{1,2,0:T(8,128)(2,1)}), bf16[16,1024,128]{1,2,0:T(8,128)(2,1)}, u32[]{:S(2)}, u32[]{:S(2)}) async-start(bf16[16,1024,128]{1,2,0:T(8,128)(2,1)} %stack.2), calls=%async_computation | async-start | bytes 8388608 | tf_op jit(solution)/shard_map/all_to_all | solution.py:36
  22.2 112.3 %all-gather.5.cloned.1.call-start = ((), (), s32[]{:S(2)}) async-start(), calls=%async_computation.4 | async-start | bytes 4456448 | tf_op jit(solution)/shard_map/all_gather | solution.py:43
  23.0 202.3 %reduce-scatter.4.cloned.1.call-start = ((), (), s32[]{:S(2)}) async-start(), calls=%async_computation.5 | async-start | bytes 8912896
  92.2 12.1 %copy-start = (bf16[1536,4096]{1,0:T(8,128)(2,1)S(1)}, bf16[1536,4096]{1,0:T(8,128)(2,1)}, u32[]{:S(2)}) copy-start(bf16[1536,4096]{1,0:T(8,128)(2,1)} %all-gather.3.cloned.1.call-done) | copy-start | bytes 37748740
  102.6 1.7 copy-start.2
  134.1 1.9 copy-start.3
Sparse Core Ops, SparseCore 0:
  10.1 70.8 all-gather.2
  83.1 51.3 all-gather.4
  137.9 84.4 reduce-scatter.3
